TPU v7x, 32 devices: a whole 2x2x4 slice. The times are simulated.
32 devices in a mesh: sp: 16 (over z, y, x), tp: 2 (over core).
Axes of the slice: x: 2, y: 2, z: 4, core: 2. Of those that a mesh axis runs over, the one named last changes fastest.
Arguments:
- mixer_in: bfloat16 [8192, 1024], P('sp', 'tp'), may hold values from -6 to 6
- residual: bfloat16 [8192, 2048], P(('sp', 'tp')), may hold values from -6 to 6
- decay_real: float32 [64, 64], P('tp'), may hold values from -2 to 0, as said below
- decay_imag: float32 [64, 64], P('tp'), may hold values from 1 to 200
- log_step: float32 [64], P('tp'), may hold values from -3.9 to -2.5
- in_real: float32 [64, 64, 16], P('tp'), may hold values from -1 to 1
- in_imag: float32 [64, 64, 16], P('tp'), may hold values from -1 to 1
- output_real: float32 [64, 16, 64], P('tp'), may hold values from -0.5 to 0.5
- output_imaginary: float32 [64, 16, 64], P('tp'), may hold values from -0.5 to 0.5
- skip: float32 [1024], P('tp'), may hold values from -4 to 4
- out_proj: bfloat16 [1024, 2048], P('tp'), may hold values from -0.1875 to 0.1875
- norm_gain: float32 [2048], replicated, may hold values from 0.1 to 1.9
- w_gate: bfloat16 [2048, 5632], P('sp', 'tp'), may hold values from -0.125 to 0.125
- w_up: bfloat16 [2048, 5632], P('sp', 'tp'), may hold values from -0.125 to 0.125
- w_down: bfloat16 [5632, 2048], P('tp', 'sp'), may hold values from -0.078125 to 0.078125
Outputs:
- output: bfloat16 [8192, 2048], P(('sp', 'tp'))
Inputs may be any that keep to these rules, and one draw needn't show every extreme that they name: `decay_real`: every entry is negative.
All inputs are finite; a program needn't handle non-finite values.
Results may differ from a plain program's by a relative error of at most 0.02.
Values may be sent and summed in bfloat16 or wider, within the bound.
A program may use at most 128 MiB of HBM per device.

v0:
```python
import jax
import jax.numpy as jnp
from jax import lax
from jax.sharding import PartitionSpec as P


def prefix(value, axis, join, neutral):
    count, mine = (lax.axis_size(axis), lax.axis_index(axis))
    pieces = jax.tree.map(lambda part: lax.all_gather(part, axis), value)
    subtotal = jax.tree.map(
        lambda part, zero: jnp.full_like(part, 0) + jnp.asarray(zero, part.dtype), value, neutral
    )

    def step(position, subtotal):
        longer = join(subtotal, jax.tree.map(lambda part: part[position], pieces))
        return jax.tree.map(lambda new, old: jnp.where(position < mine, new, old), longer, subtotal)

    return lax.fori_loop(0, count - 1, step, subtotal)


def discrete(decay_real, decay_imag, log_step, in_real, in_imag):
    step_size = jnp.exp(log_step)[:, None]
    magnitude = jnp.exp(decay_real * step_size)
    angle = decay_imag * step_size
    power_re = magnitude * jnp.cos(angle)
    power_im = magnitude * jnp.sin(angle)
    denom = decay_real * decay_real + decay_imag * decay_imag
    ratio_re = ((power_re - 1.0) * decay_real + power_im * decay_imag) / denom
    ratio_im = (power_im * decay_real - (power_re - 1.0) * decay_imag) / denom
    drive_re = ratio_re[..., None] * in_real - ratio_im[..., None] * in_imag
    drive_im = ratio_re[..., None] * in_imag + ratio_im[..., None] * in_real
    return (power_re, power_im, drive_re, drive_im)


def combine(earlier, later):
    ar1, ai1, br1, bi1 = earlier
    ar2, ai2, br2, bi2 = later
    return (
        ar2 * ar1 - ai2 * ai1,
        ar2 * ai1 + ai2 * ar1,
        ar2 * br1 - ai2 * bi1 + br2,
        ar2 * bi1 + ai2 * br1 + bi2,
    )


def spread_blocks(matrix):
    groups = matrix.shape[0]
    unit_blocks = jnp.eye(groups, dtype=jnp.float32)[:, None, :, None]
    turned = jnp.transpose(matrix, (0, 2, 1))[:, :, None, :]
    return (unit_blocks * turned).reshape(groups * matrix.shape[2], groups * matrix.shape[1])


def local_states(power_re, power_im, drive_re, drive_im):
    rows, flat_size = drive_re.shape
    span = 8
    blocks = rows // span
    dr = drive_re.reshape(blocks, span, flat_size)
    di = drive_im.reshape(blocks, span, flat_size)
    cur_re = dr[:, 0]
    cur_im = di[:, 0]
    inner_re = [cur_re]
    inner_im = [cur_im]
    lift_re = [power_re]
    lift_im = [power_im]
    for index in range(1, span):
        cur_re, cur_im = (
            power_re * cur_re - power_im * cur_im + dr[:, index],
            power_re * cur_im + power_im * cur_re + di[:, index],
        )
        inner_re.append(cur_re)
        inner_im.append(cur_im)
        prev_re, prev_im = (lift_re[-1], lift_im[-1])
        lift_re.append(power_re * prev_re - power_im * prev_im)
        lift_im.append(power_re * prev_im + power_im * prev_re)
    inner_re = jnp.stack(inner_re, axis=1)
    inner_im = jnp.stack(inner_im, axis=1)
    lift_re = jnp.concatenate(lift_re, axis=0)[None]
    lift_im = jnp.concatenate(lift_im, axis=0)[None]
    block_re = jnp.broadcast_to(lift_re[0, span - 1][None], (blocks, flat_size))
    block_im = jnp.broadcast_to(lift_im[0, span - 1][None], (blocks, flat_size))
    totals = (block_re, block_im, cur_re, cur_im)
    distance = 1
    while distance < blocks:
        ones = jnp.ones((distance, flat_size), jnp.float32)
        zeros = jnp.zeros((distance, flat_size), jnp.float32)
        moved = (
            jnp.concatenate([ones, totals[0][:-distance]], axis=0),
            jnp.concatenate([zeros, totals[1][:-distance]], axis=0),
            jnp.concatenate([zeros, totals[2][:-distance]], axis=0),
            jnp.concatenate([zeros, totals[3][:-distance]], axis=0),
        )
        totals = combine(moved, totals)
        distance = distance * 2
    one_row = jnp.ones((1, flat_size), jnp.float32)
    zero_row = jnp.zeros((1, flat_size), jnp.float32)
    before_a_re = jnp.concatenate([one_row, totals[0][:-1]], axis=0)[:, None]
    before_a_im = jnp.concatenate([zero_row, totals[1][:-1]], axis=0)[:, None]
    before_re = jnp.concatenate([zero_row, totals[2][:-1]], axis=0)[:, None]
    before_im = jnp.concatenate([zero_row, totals[3][:-1]], axis=0)[:, None]
    state_real = inner_re + lift_re * before_re - lift_im * before_im
    state_imaginary = inner_im + lift_re * before_im + lift_im * before_re
    pw_re = lift_re * before_a_re - lift_im * before_a_im
    pw_im = lift_re * before_a_im + lift_im * before_a_re
    summary = (totals[0][-1], totals[1][-1], totals[2][-1], totals[3][-1])
    return (
        pw_re.reshape(rows, flat_size),
        pw_im.reshape(rows, flat_size),
        state_real.reshape(rows, flat_size),
        state_imaginary.reshape(rows, flat_size),
        summary,
    )


def on_device(
    mixer_in,
    residual,
    decay_real,
    decay_imag,
    log_step,
    in_real,
    in_imag,
    output_real,
    output_imaginary,
    skip,
    out_proj,
    norm_gain,
    w_gate,
    w_up,
    w_down,
):
    highest_precision = lax.Precision.HIGHEST
    power_re, power_im, bar_re, bar_im = discrete(
        decay_real, decay_imag, log_step, in_real, in_imag
    )
    flat_size = decay_real.shape[0] * decay_real.shape[1]
    read_in = jnp.concatenate([spread_blocks(bar_re), spread_blocks(bar_im)], axis=1)
    signal = mixer_in.astype(jnp.float32)
    drive = jnp.dot(signal, read_in, precision=highest_precision)
    drive_re = drive[:, :flat_size]
    drive_im = drive[:, flat_size:]
    pw_re, pw_im, state_real, state_imaginary, summary = local_states(
        power_re.reshape(1, flat_size), power_im.reshape(1, flat_size), drive_re, drive_im
    )
    zero_line = jnp.zeros((flat_size,), jnp.float32)
    identity = (jnp.ones((flat_size,), jnp.float32), zero_line, zero_line, zero_line)
    _, _, hold_re, hold_im = prefix(summary, "sp", combine, identity)
    state_real = state_real + pw_re * hold_re[None] - pw_im * hold_im[None]
    state_imaginary = state_imaginary + pw_re * hold_im[None] + pw_im * hold_re[None]
    read_out = jnp.concatenate(
        [spread_blocks(output_real), -spread_blocks(output_imaginary)], axis=0
    )
    mixed_before_norm = jnp.dot(
        jnp.concatenate([state_real, state_imaginary], axis=1),
        read_out,
        precision=highest_precision,
    )
    mixed_before_norm = mixed_before_norm + skip[None] * signal
    activated = jax.nn.gelu(mixed_before_norm).astype(jnp.bfloat16)
    partial_value = jnp.dot(activated, out_proj, preferred_element_type=jnp.float32).astype(
        jnp.bfloat16
    )
    mixed = lax.psum_scatter(
        lax.optimization_barrier(partial_value).astype(jnp.float32).astype(jnp.bfloat16),
        "tp",
        scatter_dimension=0,
        tiled=True,
    )
    carried = residual.astype(jnp.float32) + mixed.astype(jnp.float32)
    scale = lax.rsqrt(jnp.mean(carried * carried, axis=-1, keepdims=True) + 1e-06)
    normed = (carried * scale * norm_gain).astype(jnp.bfloat16)
    full_rows = lax.all_gather(normed, "tp", axis=0, tiled=True)
    gate = jnp.dot(
        full_rows,
        lax.all_gather(w_gate, "sp", axis=0, tiled=True),
        preferred_element_type=jnp.float32,
    )
    up = jnp.dot(
        full_rows,
        lax.all_gather(w_up, "sp", axis=0, tiled=True),
        preferred_element_type=jnp.float32,
    )
    down_columns = lax.all_gather(w_down, "sp", axis=1, tiled=True)
    hidden = (jax.nn.silu(gate) * up).astype(jnp.bfloat16)
    partial_value = jnp.dot(hidden, down_columns, preferred_element_type=jnp.float32).astype(
        jnp.bfloat16
    )
    down = lax.psum_scatter(
        lax.optimization_barrier(partial_value).astype(jnp.float32).astype(jnp.bfloat16),
        "tp",
        scatter_dimension=0,
        tiled=True,
    )
    return (carried + 0.5 * down.astype(jnp.float32)).astype(jnp.bfloat16)


def solution(mesh):
    return jax.shard_map(
        on_device,
        mesh=mesh,
        in_specs=(
            P("sp", "tp"),
            P(("sp", "tp"), None),
            P("tp", None),
            P("tp", None),
            P("tp"),
            P("tp", None, None),
            P("tp", None, None),
            P("tp", None, None),
            P("tp", None, None),
            P("tp"),
            P("tp", None),
            P(),
            P("sp", "tp"),
            P("sp", "tp"),
            P("tp", "sp"),
        ),
        out_specs=P(("sp", "tp"), None),
        check_vma=False,
    )
```

profile of v0, /device:TPU:0, one launch (start us, length us, event | category | flops | bytes accessed | tf_op | source)
XLA Modules:
  0.0 897.7 jit_solution(369592521946466958)
XLA Ops:
  9.7 8.3 broadcast_multiply_fusion.2
  18.1 7.8 mul.1865
  25.9 7.9 mul.1870
  33.8 10.5 %fusion.11 = f32[512,4096]{1,0:T(8,128)S(1)} fusion(bf16[512,512]{1,0:T(8,128)(2,1)S(1)} %copy-done.39, f32[512,2048]{1,0:T(8,128)} %mul.1870, f32[512,2048]{1,0:T(8,128)} %mul.1865), kind=kOutput, calls=%fused_computation.18 | convolution fusion | flops 12886999040 | bytes 17301504 | tf_op jit(solution)/shard_map/dot_general | solution.py:138
  89.2 43.1 %all-gather.2 = f32[16,1,2048]{2,1,0:T(1,128)S(1)} all-gather(f32[1,1,2048]{2,1,0:T(1,128)S(1)} %slice_bitcast_fusion.3), channel_id=1, replica_groups=mesh['sp'=16,'tp'=2] {'sp'}, dimensions={0}, use_global_device_ids=true | all-gather | bytes 139264 | tf_op jit(solution)/shard_map/all_gather | solution.py:9
  132.3 36.1 %all-gather.1 = f32[16,1,2048]{2,1,0:T(1,128)S(1)} all-gather(f32[1,1,2048]{2,1,0:T(1,128)S(1)} %slice_bitcast_fusion.4), channel_id=1, replica_groups=mesh['sp'=16,'tp'=2] {'sp'}, dimensions={0}, use_global_device_ids=true | all-gather | bytes 139264 | tf_op jit(solution)/shard_map/all_gather | solution.py:9
  168.5 38.2 %all-gather = f32[16,1,2048]{2,1,0:T(1,128)S(1)} all-gather(f32[1,1,2048]{2,1,0:T(1,128)S(1)} %slice_bitcast_fusion.5), channel_id=1, replica_groups=mesh['sp'=16,'tp'=2] {'sp'}, dimensions={0}, use_global_device_ids=true | all-gather | bytes 139264 | tf_op jit(solution)/shard_map/all_gather | solution.py:9
  207.5 36.2 %all-gather.3 = f32[16,1,2048]{2,1,0:T(1,128)S(1)} all-gather(f32[1,1,2048]{2,1,0:T(1,128)S(1)} %slice_bitcast_fusion.2), channel_id=1, replica_groups=mesh['sp'=16,'tp'=2] {'sp'}, dimensions={0}, use_global_device_ids=true | all-gather | bytes 139264 | tf_op jit(solution)/shard_map/all_gather | solution.py:9
  244.3 26.6 %while.16 = (s32[]{:T(128)}, f32[2048]{0:T(1024)S(1)}, f32[2048]{0:T(1024)S(1)}, s32[]{:T(128)}, f32[16,2048]{1,0:T(8,128)}, /*index=5*/f32[16,2048]{1,0:T(8,128...) while((s32[]{:T(128)}, f32[2048]{0:T(1024)S(1)}, f32[2048]{0:T(1024)S(1)}, ...), condition=%wide.region_1.2_spmd.clone, body=%wide.region_0.1_spmd.clone.sunk | while | flops 24580 | bytes 131201 | solution.py:18
  284.8 8.1 broadcast_multiply_fusion
  293.0 7.8 mul.2031
  300.8 7.8 neg.11
  310.5 11.9 %stack.5 = f32[64,8,2048]{2,1,0:T(8,128)} concatenate(f32[64,1,2048]{2,1,0:T(1,128)S(1)} %get-tuple-element.246, f32[64,1,2048]{2,1,0:T(1,128)} %copy.106, f32[64,1,2048]{2,1,0:T(1,128)} %copy.107, f32[64,1,2048]{2,1,0:T(1,128)} %copy.108, f32[64,1,2048]{2,1,0:T(1,128)} %copy.109, f32[64,1,2048]{2,1,0:T(1,128)} %copy.110, f32[64,1,2048]{2,1,0:T(1,128)} %copy.111, ...), dimensions={1} | concatenate | bytes 8388608 | tf_op jit(solution)/shard_map/stack | solution.py:76
  322.4 12.0 %stack.4 = f32[64,8,2048]{2,1,0:T(8,128)} concatenate(f32[64,1,2048]{2,1,0:T(1,128)S(1)} %get-tuple-element.248, f32[64,1,2048]{2,1,0:T(1,128)} %copy.98, f32[64,1,2048]{2,1,0:T(1,128)} %copy.99, f32[64,1,2048]{2,1,0:T(1,128)} %copy.100, f32[64,1,2048]{2,1,0:T(1,128)} %copy.101, f32[64,1,2048]{2,1,0:T(1,128)} %copy.102, f32[64,1,2048]{2,1,0:T(1,128)} %copy.103, ...), dimensions={1} | concatenate | bytes 8388608 | tf_op jit(solution)/shard_map/stack | solution.py:75
  334.4 7.0 fusion.15
  342.3 16.5 %fusion.24 = bf16[512,512]{1,0:T(8,128)(2,1)S(1)} fusion(bf16[512,512]{1,0:T(8,128)(2,1)S(1)} %copy-done.40, f32[2048,512]{0,1:T(8,128)S(1)} %copy-done.22, f32[2048,512]{0,1:T(8,128)S(1)} %copy-done.21, f32[512,2048]{1,0:T(8,128)} %get-tuple-element.258, f32[512,2048]{1,0:T(8,128)S(1)} %get-tuple-element.257, f32[512]{0:T(512)S(1)} %copy-done.50), kind=kOutput, calls=%fused_computation.49 | convolution fusion | flops 12892241920 | bytes 17827840 | tf_op jit(solution)/shard_map/dot_general | solution.py:152
  361.5 7.6 reduce-scatter.3.cloned.1.call-done
  375.3 10.1 %all-gather.9.cloned.1.call-done = bf16[512,2048]{1,0:T(8,128)(2,1)} async-done(((bf16[256,2048]{1,0:T(8,128)(2,1)}), bf16[512,2048]{1,0:T(8,128)(2,1)}) %all-gather.9.cloned.1.call-update) | async-done | bytes 2097168 | tf_op jit(solution)/shard_map/all_gather | solution.py:171
  385.4 145.4 %all-gather.11.cloned.1.call-done = bf16[2048,2816]{1,0:T(8,128)(2,1)} async-done(((bf16[128,2816]{1,0:T(8,128)(2,1)}), bf16[2048,2816]{1,0:T(8,128)(2,1)}) %all-gather.11.cloned.1.call-update) | async-done | bytes 11534352 | tf_op jit(solution)/shard_map/all_gather | solution.py:174
  530.8 12.7 %fusion.63 = f32[512,2816]{1,0:T(8,128)} fusion(bf16[512,2048]{1,0:T(8,128)(2,1)} %all-gather.9.cloned.1.call-done, bf16[2048,2816]{1,0:T(8,128)(2,1)} %all-gather.11.cloned.1.call-done), kind=kOutput, calls=%fused_computation.183 | convolution fusion | flops 5905580032 | bytes 19398656 | tf_op jit(solution)/shard_map/dot_general | solution.py:172
  543.5 129.6 %all-gather.13.cloned.1.call-done = bf16[2048,2816]{1,0:T(8,128)(2,1)} async-done(((bf16[128,2816]{1,0:T(8,128)(2,1)}), bf16[2048,2816]{1,0:T(8,128)(2,1)}) %all-gather.13.cloned.1.call-update) | async-done | bytes 11534352 | tf_op jit(solution)/shard_map/all_gather | solution.py:179
  673.0 182.8 %all-gather.15.cloned.1.call-done = bf16[2816,2048]{1,0:T(8,128)(2,1)} async-done(((bf16[2816,128]{1,0:T(8,128)(2,1)}), bf16[2816,2048]{1,0:T(8,128)(2,1)}) %all-gather.15.cloned.1.call-update) | async-done | bytes 11534352 | tf_op jit(solution)/shard_map/all_gather | solution.py:182
  855.8 23.4 %convolution_convert_fusion = bf16[512,2048]{1,0:T(8,128)(2,1)} fusion(bf16[2816,2048]{1,0:T(8,128)(2,1)} %all-gather.15.cloned.1.call-done, f32[512,2816]{1,0:T(8,128)} %fusion.63, bf16[512,2048]{1,0:T(8,128)(2,1)} %all-gather.9.cloned.1.call-done, bf16[2048,2816]{1,0:T(8,128)(2,1)} %all-gather.13.cloned.1.call-done), kind=kOutput, calls=%fused_computation.35 | convolution fusion | flops 11820859392 | bytes 33030144 | tf_op jit(solution)/shard_map/dot_general | solution.py:184
  879.2 8.1 reduce-scatter.5.cloned.1.call-done
  (240 shorter events, 103.5 us)
Async XLA Ops:
  6.5 352.3 %copy-start = (bf16[512,2048]{1,0:T(8,128)(2,1)S(1)}, bf16[512,2048]{1,0:T(8,128)(2,1)}, u32[]{:S(2)}) copy-start(bf16[512,2048]{1,0:T(8,128)(2,1)} %param.27) | copy-start | bytes 6291460
  6.5 362.6 %reduce-scatter.3.cloned.1.call-start = ((), (), s32[]{:S(2)}) async-start(), calls=%async_computation.2 | async-start | bytes 3145728 | tf_op jit(solution)/shard_map/reduce_scatter | solution.py:162
  6.5 11.5 %copy-start.47 = (f32[32,32]{0,1:T(8,128)}, f32[32,32]{0,1:T(8,128)S(1)}, u32[]{:S(2)}) copy-start(f32[32,32]{0,1:T(8,128)S(1)} %fusion.52) | copy-start | bytes 12292
  76.0 12.5 %copy-start.24 = (f32[64,2048]{1,0:T(8,128)S(1)}, f32[64,2048]{1,0:T(8,128)}, u32[]{:S(2)}) copy-start(f32[64,2048]{1,0:T(8,128)} %fusion.38) | copy-start | bytes 1572868
  76.0 12.5 %copy-start.23 = (f32[64,2048]{1,0:T(8,128)S(1)}, f32[64,2048]{1,0:T(8,128)}, u32[]{:S(2)}) copy-start(f32[64,2048]{1,0:T(8,128)} %get-tuple-element.206) | copy-start | bytes 1572868
  76.0 12.5 %copy-start.9 = (f32[64,2048]{1,0:T(8,128)S(1)}, f32[64,2048]{1,0:T(8,128)}, u32[]{:S(2)}) copy-start(f32[64,2048]{1,0:T(8,128)} %copy-done.8) | copy-start | bytes 1572868
  76.0 12.5 %copy-start.11 = (f32[64,2048]{1,0:T(8,128)S(1)}, f32[64,2048]{1,0:T(8,128)}, u32[]{:S(2)}) copy-start(f32[64,2048]{1,0:T(8,128)} %copy-done.10) | copy-start | bytes 1572868
  76.0 12.5 %copy-start.38 = (f32[48,2048]{1,0:T(8,128)S(1)}, f32[48,2048]{1,0:T(8,128)}, u32[]{:S(2)}) copy-start(f32[48,2048]{1,0:T(8,128)} %slice.234) | copy-start | bytes 1179652
  88.8 118.6 %copy-start.25 = (f32[64,2048]{1,0:T(8,128)}, f32[64,2048]{1,0:T(8,128)S(1)}, u32[]{:S(2)}) copy-start(f32[64,2048]{1,0:T(8,128)S(1)} %get-tuple-element.203) | copy-start | bytes 1572868
  89.1 118.3 %copy-start.26 = (f32[64,2048]{1,0:T(8,128)}, f32[64,2048]{1,0:T(8,128)S(1)}, u32[]{:S(2)}) copy-start(f32[64,2048]{1,0:T(8,128)S(1)} %get-tuple-element.262) | copy-start | bytes 1572868
  89.1 154.5 %copy-start.27 = (f32[64,2048]{1,0:T(8,128)}, f32[64,2048]{1,0:T(8,128)S(1)}, u32[]{:S(2)}) copy-start(f32[64,2048]{1,0:T(8,128)S(1)} %get-tuple-element.261) | copy-start | bytes 1572868
  89.1 154.5 %copy-start.28 = (f32[64,2048]{1,0:T(8,128)}, f32[64,2048]{1,0:T(8,128)S(1)}, u32[]{:S(2)}) copy-start(f32[64,2048]{1,0:T(8,128)S(1)} %get-tuple-element.267) | copy-start | bytes 1572868
  271.0 12.3 %copy-start.31 = (f32[64,1,2048]{2,0,1:T(8,128)S(1)}, f32[64,1,2048]{2,0,1:T(8,128)}, u32[]{:S(2)}) copy-start(f32[64,1,2048]{2,0,1:T(8,128)} %get-tuple-element.199) | copy-start | bytes 1572868
  271.0 13.6 %copy-start.45 = (f32[32,16,64]{2,1,0:T(8,128)S(1)}, f32[32,16,64]{2,1,0:T(8,128)}, u32[]{:S(2)}) copy-start(f32[32,16,64]{2,1,0:T(8,128)} %param.24) | copy-start | bytes 393220
  273.0 11.7 %copy-start.46 = (f32[32,16,64]{2,1,0:T(8,128)S(1)}, f32[32,16,64]{2,1,0:T(8,128)}, u32[]{:S(2)}) copy-start(f32[32,16,64]{2,1,0:T(8,128)} %param.25) | copy-start | bytes 393220
  273.0 11.8 %copy-start.48 = (f32[32,32]{0,1:T(8,128)S(1)}, f32[32,32]{0,1:T(8,128)}, u32[]{:S(2)}) copy-start(f32[32,32]{0,1:T(8,128)} %copy-done.47) | copy-start | bytes 12292
  322.4 12.0 %copy-start.37 = (f32[64,2048]{1,0:T(8,128)S(1)}, f32[64,2048]{1,0:T(8,128)}, u32[]{:S(2)}) copy-start(f32[64,2048]{1,0:T(8,128)} %concatenate.124) | copy-start | bytes 1572868
  322.4 12.0 %copy-start.42 = (f32[8,2048]{1,0:T(8,128)S(1)}, f32[8,2048]{1,0:T(8,128)}, u32[]{:S(2)}) copy-start(f32[8,2048]{1,0:T(8,128)} %copy-done.41) | copy-start | bytes 196612
  322.4 12.0 %copy-start.44 = (f32[8,2048]{1,0:T(8,128)S(1)}, f32[8,2048]{1,0:T(8,128)}, u32[]{:S(2)}) copy-start(f32[8,2048]{1,0:T(8,128)} %copy-done.43) | copy-start | bytes 196612
  361.4 23.9 %all-gather.9.cloned.1.call-start = ((), (), s32[]{:S(2)}) async-start(), calls=%async_computation.3 | async-start | bytes 3145728 | tf_op jit(solution)/shard_map/all_gather | solution.py:171
  373.4 157.4 %all-gather.11.cloned.1.call-start = ((), (), s32[]{:S(2)}) async-start(), calls=%async_computation.4 | async-start | bytes 12255232 | tf_op jit(solution)/shard_map/all_gather | solution.py:174
  374.1 298.9 %all-gather.13.cloned.1.call-start = ((), (), s32[]{:S(2)}) async-start(), calls=%async_computation.5 | async-start | bytes 12255232 | tf_op jit(solution)/shard_map/all_gather | solution.py:179
  374.7 481.1 %all-gather.15.cloned.1.call-start = ((), (), s32[]{:S(2)}) async-start(), calls=%async_computation.6 | async-start | bytes 12255232 | tf_op jit(solution)/shard_map/all_gather | solution.py:182
  375.3 512.1 %reduce-scatter.5.cloned.1.call-start = ((), (), s32[]{:S(2)}) async-start(), calls=%async_computation.7 | async-start | bytes 3145728 | tf_op jit(solution)/shard_map/reduce_scatter | solution.py:187
  (33 other events, 230.0 us)
Sparse Core Ops, SparseCore 0:
  361.6 7.4 reduce-scatter.2
  373.5 11.8 all-gather.8
  388.1 142.5 all-gather.10
  533.4 139.5 all-gather.12
  675.6 180.2 all-gather.14
  879.3 7.9 reduce-scatter.4
where the time goes:
time: 910 us; the launch traced here: 898 us
  waiting for transfers between devices  485 us (53%)
  blocking collectives  154 us (17%)
  local copies, waits for them, and re-layouts  123 us (14%)
  matrix products  65.6 us (7%)
  other arithmetic  54.9 us (6%)
  between operations  14.7 us (2%)
    all_gather x1, waiting for transfers between devices, on_device(): down_columns = lax.all_gather(w_down, 'sp', axis=1, tiled=True)  183 us
    all_gather x4, blocking collectives, prefix(): pieces = jax.tree.map(lambda part: lax.all_gather(part, axis), value)  154 us
    all_gather x1, waiting for transfers between devices, on_device(): lax.all_gather(w_gate, 'sp', axis=0, tiled=True)  145 us
    all_gather x1, waiting for transfers between devices, on_device(): lax.all_gather(w_up, 'sp', axis=0, tiled=True)  130 us
    dynamic_slice x30, local copies, waits for them, and re-layouts, step(): longer = join(subtotal, jax.tree.map(lambda part: part[position], pieces))  25.8 us
    mul x3, local copies, waits for them, and re-layouts, spread_blocks(): unit_blocks * turned  23.5 us
    dot_general x1, matrix products, on_device(): jnp.dot(hidden, down_columns, preferred_element_type=jnp.float32)  23.4 us
  transfers between devices with their start and end apart: 6, of which 6 were waited for; matrix products, arithmetic and copies ran while one was open for 1% of the time, Pallas kernels for 0%

commit v1 on v0

--- a/solution.py
+++ b/solution.py
@@ -2,6 +2,23 @@
 import jax.numpy as jnp
 from jax import lax
 from jax.sharding import PartitionSpec as P
+
+
+def joined_along(blocks, dim):
+    shape = list(blocks.shape[1:])
+    shape[dim] *= blocks.shape[0]
+    return jnp.moveaxis(blocks, 0, dim).reshape(shape)
+
+
+def collect(x, axis, dim):
+    size = lax.axis_size(axis)
+    right = [(i, (i + 1) % size) for i in range(size)]
+    blocks = [x]
+    while len(blocks) < size:
+        blocks.append(lax.ppermute(blocks[-1], axis, right))
+    mine = lax.axis_index(axis)
+    blocks = jnp.stack(blocks)[(mine - jnp.arange(size)) % size]
+    return joined_along(blocks, dim)
 
 
 def prefix(value, axis, join, neutral):
@@ -179,7 +196,7 @@
         lax.all_gather(w_up, "sp", axis=0, tiled=True),
         preferred_element_type=jnp.float32,
     )
-    down_columns = lax.all_gather(w_down, "sp", axis=1, tiled=True)
+    down_columns = collect(w_down, "sp", 1)
     hidden = (jax.nn.silu(gate) * up).astype(jnp.bfloat16)
     partial_value = jnp.dot(hidden, down_columns, preferred_element_type=jnp.float32).astype(
         jnp.bfloat16

time: 910 us -> 959 us (1.054)
  local copies, waits for them, and re-layouts: 123 us -> 168 us
    ppermute x0 -> x15, waiting for transfers between devices: none -> 463 us  [collect(): blocks.append(lax.ppermute(blocks[-1], axis, right))]
    all_gather x1 -> x0, waiting for transfers between devices: 183 us -> none  [on_device(): down_columns = lax.all_gather(w_down, 'sp', axis=1, tiled=True)]
    all_gather x1, waiting for transfers between devices: 145 us -> 0.01 us  [on_device(): lax.all_gather(w_gate, 'sp', axis=0, tiled=True)]
    all_gather x1, waiting for transfers between devices: 130 us -> 0.01 us  [on_device(): lax.all_gather(w_up, 'sp', axis=0, tiled=True)]
    transpose x0 -> x1, local copies, waits for them, and re-layouts: none -> 14.9 us  [joined_along(): return jnp.moveaxis(blocks, 0, dim).reshape(shape)]
    unnamed x110 -> x109, local copies, waits for them, and re-layouts: 3.38 us -> 17.7 us
    gather x0 -> x1, local copies, waits for them, and re-layouts: none -> 10.4 us  [collect(): blocks = jnp.stack(blocks)[(mine - jnp.arange(size)) % size]]
    all_gather x1, waiting for transfers between devices: 10.1 us -> 0.01 us  [on_device(): full_rows = lax.all_gather(normed, 'tp', axis=0, tiled=True)]
  transfers between devices with their start and end apart: 6 -> 20, of which waited for: 6 -> 17; matrix products, arithmetic and copies ran while one was open for 1% -> 6% of each run, Pallas kernels for 0% -> 0%
where the time goes in v1:
time: 959 us; the launch traced here: 945 us
  waiting for transfers between devices  479 us (50%)
  local copies, waits for them, and re-layouts  168 us (18%)
  blocking collectives  154 us (16%)
  matrix products  69.4 us (7%)
  other arithmetic  57.2 us (6%)
  between operations  14.3 us (1%)
    ppermute x15, waiting for transfers between devices, collect(): blocks.append(lax.ppermute(blocks[-1], axis, right))  463 us
    all_gather x4, blocking collectives, prefix(): pieces = jax.tree.map(lambda part: lax.all_gather(part, axis), value)  154 us
    dot_general x1, matrix products, on_device(): jnp.dot(hidden, down_columns, preferred_element_type=jnp.float32)  27.4 us
    dynamic_slice x30, local copies, waits for them, and re-layouts, step(): longer = join(subtotal, jax.tree.map(lambda part: part[position], pieces))  26.7 us
    mul x3, local copies, waits for them, and re-layouts, spread_blocks(): unit_blocks * turned  23.5 us
  transfers between devices with their start and end apart: 20, of which 17 were waited for; matrix products, arithmetic and copies ran while one was open for 6% of the time, Pallas kernels for 0%

profile of v1, /device:TPU:0, one launch (start us, length us, event | category | flops | bytes accessed | tf_op | source)
XLA Modules:
  0.0 945.3 jit_solution(1930564569433427898)
XLA Ops:
  92.6 43.2 %all-gather.2 = f32[16,1,2048]{2,1,0:T(1,128)S(1)} all-gather(f32[1,1,2048]{2,1,0:T(1,128)S(1)} %slice_bitcast_fusion.3), channel_id=1, replica_groups=mesh['sp'=16,'tp'=2] {'sp'}, dimensions={0}, use_global_device_ids=true | all-gather | bytes 139264 | tf_op jit(solution)/shard_map/all_gather | solution.py:26
  136.6 36.2 %all-gather.1 = f32[16,1,2048]{2,1,0:T(1,128)S(1)} all-gather(f32[1,1,2048]{2,1,0:T(1,128)S(1)} %slice_bitcast_fusion.4), channel_id=1, replica_groups=mesh['sp'=16,'tp'=2] {'sp'}, dimensions={0}, use_global_device_ids=true | all-gather | bytes 139264 | tf_op jit(solution)/shard_map/all_gather | solution.py:26
  173.5 38.1 %all-gather = f32[16,1,2048]{2,1,0:T(1,128)S(1)} all-gather(f32[1,1,2048]{2,1,0:T(1,128)S(1)} %slice_bitcast_fusion.5), channel_id=1, replica_groups=mesh['sp'=16,'tp'=2] {'sp'}, dimensions={0}, use_global_device_ids=true | all-gather | bytes 139264 | tf_op jit(solution)/shard_map/all_gather | solution.py:26
  212.4 36.3 %all-gather.3 = f32[16,1,2048]{2,1,0:T(1,128)S(1)} all-gather(f32[1,1,2048]{2,1,0:T(1,128)S(1)} %slice_bitcast_fusion.2), channel_id=1, replica_groups=mesh['sp'=16,'tp'=2] {'sp'}, dimensions={0}, use_global_device_ids=true | all-gather | bytes 139264 | tf_op jit(solution)/shard_map/all_gather | solution.py:26
  249.3 27.6 %while.16 = (s32[]{:T(128)}, f32[2048]{0:T(1024)S(1)}, f32[2048]{0:T(1024)S(1)}, s32[]{:T(128)}, f32[16,2048]{1,0:T(8,128)}, /*index=5*/f32[16,2048]{1,0:T(8,128...) while((s32[]{:T(128)}, f32[2048]{0:T(1024)S(1)}, f32[2048]{0:T(1024)S(1)}, ...), condition=%wide.region_1.2_spmd.clone, body=%wide.region_0.1_spmd.clone.sunk | while | flops 24580 | bytes 131201 | solution.py:35
  350.3 16.5 %fusion.24 = bf16[512,512]{1,0:T(8,128)(2,1)S(1)} fusion(bf16[512,512]{1,0:T(8,128)(2,1)S(1)} %copy-done.32, f32[2048,512]{0,1:T(8,128)S(1)} %copy-done.19, f32[2048,512]{0,1:T(8,128)S(1)} %copy-done.18, f32[512,2048]{1,0:T(8,128)} %get-tuple-element.258, f32[512,2048]{1,0:T(8,128)S(1)} %get-tuple-element.257, f32[512]{0:T(512)S(1)} %copy-done.42), kind=kOutput, calls=%fused_computation.50 | convolution fusion | flops 12892241920 | bytes 17827840 | tf_op jit(solution)/shard_map/dot_general | solution.py:169
  384.5 20.2 %collective-permute-done = bf16[2816,128]{1,0:T(8,128)(2,1)S(1)} collective-permute-done((bf16[2816,128]{1,0:T(8,128)(2,1)S(1)}, bf16[2816,128]{1,0:T(8,128)(2,1)S(1)}, u32[]{:S(2)}, u32[]{:S(2)}) %collective-permute-start) | collective-permute-done | bytes 720928 | tf_op jit(solution)/shard_map/ppermute | solution.py:18
  404.7 35.7 %collective-permute-done.1 = bf16[2816,128]{1,0:T(8,128)(2,1)S(1)} collective-permute-done((bf16[2816,128]{1,0:T(8,128)(2,1)S(1)}, bf16[2816,128]{1,0:T(8,128)(2,1)S(1)}, u32[]{:S(2)}, u32[]{:S(2)}) %collective-permute-start.1) | collective-permute-done | bytes 720928 | tf_op jit(solution)/shard_map/ppermute | solution.py:18
  440.4 34.3 %collective-permute-done.2 = bf16[2816,128]{1,0:T(8,128)(2,1)S(1)} collective-permute-done((bf16[2816,128]{1,0:T(8,128)(2,1)S(1)}, bf16[2816,128]{1,0:T(8,128)(2,1)S(1)}, u32[]{:S(2)}, u32[]{:S(2)}) %collective-permute-start.2) | collective-permute-done | bytes 720928 | tf_op jit(solution)/shard_map/ppermute | solution.py:18
  474.8 32.9 %collective-permute-done.3 = bf16[2816,128]{1,0:T(8,128)(2,1)S(1)} collective-permute-done((bf16[2816,128]{1,0:T(8,128)(2,1)S(1)}, bf16[2816,128]{1,0:T(8,128)(2,1)S(1)}, u32[]{:S(2)}, u32[]{:S(2)}) %collective-permute-start.3) | collective-permute-done | bytes 720928 | tf_op jit(solution)/shard_map/ppermute | solution.py:18
  507.7 37.2 %collective-permute-done.4 = bf16[2816,128]{1,0:T(8,128)(2,1)S(1)} collective-permute-done((bf16[2816,128]{1,0:T(8,128)(2,1)S(1)}, bf16[2816,128]{1,0:T(8,128)(2,1)S(1)}, u32[]{:S(2)}, u32[]{:S(2)}) %collective-permute-start.4) | collective-permute-done | bytes 720928 | tf_op jit(solution)/shard_map/ppermute | solution.py:18
  544.9 37.6 %collective-permute-done.5 = bf16[2816,128]{1,0:T(8,128)(2,1)S(1)} collective-permute-done((bf16[2816,128]{1,0:T(8,128)(2,1)S(1)}, bf16[2816,128]{1,0:T(8,128)(2,1)S(1)}, u32[]{:S(2)}, u32[]{:S(2)}) %collective-permute-start.5) | collective-permute-done | bytes 720928 | tf_op jit(solution)/shard_map/ppermute | solution.py:18
  582.5 38.0 %collective-permute-done.6 = bf16[2816,128]{1,0:T(8,128)(2,1)S(1)} collective-permute-done((bf16[2816,128]{1,0:T(8,128)(2,1)S(1)}, bf16[2816,128]{1,0:T(8,128)(2,1)S(1)}, u32[]{:S(2)}, u32[]{:S(2)}) %collective-permute-start.6) | collective-permute-done | bytes 720928 | tf_op jit(solution)/shard_map/ppermute | solution.py:18
  621.4 24.9 %collective-permute-done.7 = bf16[2816,128]{1,0:T(8,128)(2,1)S(1)} collective-permute-done((bf16[2816,128]{1,0:T(8,128)(2,1)S(1)}, bf16[2816,128]{1,0:T(8,128)(2,1)S(1)}, u32[]{:S(2)}, u32[]{:S(2)}) %collective-permute-start.7) | collective-permute-done | bytes 720928 | tf_op jit(solution)/shard_map/ppermute | solution.py:18
  648.2 25.1 %collective-permute-done.8 = bf16[2816,128]{1,0:T(8,128)(2,1)S(1)} collective-permute-done((bf16[2816,128]{1,0:T(8,128)(2,1)S(1)}, bf16[2816,128]{1,0:T(8,128)(2,1)S(1)}, u32[]{:S(2)}, u32[]{:S(2)}) %collective-permute-start.8) | collective-permute-done | bytes 720928 | tf_op jit(solution)/shard_map/ppermute | solution.py:18
  675.1 34.1 %collective-permute-done.9 = bf16[2816,128]{1,0:T(8,128)(2,1)S(1)} collective-permute-done((bf16[2816,128]{1,0:T(8,128)(2,1)S(1)}, bf16[2816,128]{1,0:T(8,128)(2,1)S(1)}, u32[]{:S(2)}, u32[]{:S(2)}) %collective-permute-start.9) | collective-permute-done | bytes 720928 | tf_op jit(solution)/shard_map/ppermute | solution.py:18
  710.9 26.1 %collective-permute-done.10 = bf16[2816,128]{1,0:T(8,128)(2,1)S(1)} collective-permute-done((bf16[2816,128]{1,0:T(8,128)(2,1)S(1)}, bf16[2816,128]{1,0:T(8,128)(2,1)S(1)}, u32[]{:S(2)}, u32[]{:S(2)}) %collective-permute-start.10) | collective-permute-done | bytes 720928 | tf_op jit(solution)/shard_map/ppermute | solution.py:18
  738.9 35.6 %collective-permute-done.11 = bf16[2816,128]{1,0:T(8,128)(2,1)S(1)} collective-permute-done((bf16[2816,128]{1,0:T(8,128)(2,1)S(1)}, bf16[2816,128]{1,0:T(8,128)(2,1)S(1)}, u32[]{:S(2)}, u32[]{:S(2)}) %collective-permute-start.11) | collective-permute-done | bytes 720928 | tf_op jit(solution)/shard_map/ppermute | solution.py:18
  776.3 33.2 %collective-permute-done.12 = bf16[2816,128]{1,0:T(8,128)(2,1)S(1)} collective-permute-done((bf16[2816,128]{1,0:T(8,128)(2,1)S(1)}, bf16[2816,128]{1,0:T(8,128)(2,1)S(1)}, u32[]{:S(2)}, u32[]{:S(2)}) %collective-permute-start.12) | collective-permute-done | bytes 720928 | tf_op jit(solution)/shard_map/ppermute | solution.py:18
  811.4 35.4 %collective-permute-done.13 = bf16[2816,128]{1,0:T(8,128)(2,1)S(1)} collective-permute-done((bf16[2816,128]{1,0:T(8,128)(2,1)S(1)}, bf16[2816,128]{1,0:T(8,128)(2,1)S(1)}, u32[]{:S(2)}, u32[]{:S(2)}) %collective-permute-start.13) | collective-permute-done | bytes 720928 | tf_op jit(solution)/shard_map/ppermute | solution.py:18
  848.9 13.0 %collective-permute-done.14 = bf16[2816,128]{1,0:T(8,128)(2,1)S(1)} collective-permute-done((bf16[2816,128]{1,0:T(8,128)(2,1)S(1)}, bf16[2816,128]{1,0:T(8,128)(2,1)S(1)}, u32[]{:S(2)}, u32[]{:S(2)}) %collective-permute-start.14) | collective-permute-done | bytes 720928 | tf_op jit(solution)/shard_map/ppermute | solution.py:18
  873.2 14.9 %copy.148 = bf16[2816,16,128]{0,2,1:T(8,128)(2,1)} copy(bf16[2816,16,128]{2,0,1:T(8,128)(2,1)} %bitcast.240) | data formatting | bytes 23068672 | tf_op jit(solution)/shard_map/transpose | solution.py:10
  888.2 12.5 %fusion.65 = f32[512,2816]{1,0:T(8,128)} fusion(bf16[512,2048]{1,0:T(8,128)(2,1)} %all-gather.8.cloned.1.call-done, bf16[2048,2816]{1,0:T(8,128)(2,1)} %all-gather.10.cloned.1.call-done), kind=kOutput, calls=%fused_computation.207 | convolution fusion | flops 5905580032 | bytes 19398656 | tf_op jit(solution)/shard_map/dot_general | solution.py:189
  900.6 27.4 %convolution_convert_fusion = bf16[512,2048]{1,0:T(8,128)(2,1)} fusion(bf16[2816,2048]{0,1:T(8,128)(2,1)} %bitcast.241, f32[512,2816]{1,0:T(8,128)} %fusion.65, bf16[512,2048]{1,0:T(8,128)(2,1)} %all-gather.8.cloned.1.call-done, bf16[2048,2816]{1,0:T(8,128)(2,1)} %all-gather.12.cloned.1.call-done), kind=kOutput, calls=%fused_computation.36 | convolution fusion | flops 11820859392 | bytes 33030144 | tf_op jit(solution)/shard_map/dot_general | solution.py:201
  (271 shorter events, 241.9 us)
Async XLA Ops:
  6.5 360.3 %copy-start = (bf16[512,2048]{1,0:T(8,128)(2,1)S(1)}, bf16[512,2048]{1,0:T(8,128)(2,1)}, u32[]{:S(2)}) copy-start(bf16[512,2048]{1,0:T(8,128)(2,1)} %param.27) | copy-start | bytes 6291460
  6.5 370.4 %reduce-scatter.3.cloned.1.call-start = ((), (), s32[]{:S(2)}) async-start(), calls=%async_computation.2 | async-start | bytes 3145728 | tf_op jit(solution)/shard_map/reduce_scatter | solution.py:179
  92.6 156.1 %copy-start.24 = (f32[64,2048]{1,0:T(8,128)}, f32[64,2048]{1,0:T(8,128)S(1)}, u32[]{:S(2)}) copy-start(f32[64,2048]{1,0:T(8,128)S(1)} %get-tuple-element.261) | copy-start | bytes 1572868
  92.6 156.1 %copy-start.25 = (f32[64,2048]{1,0:T(8,128)}, f32[64,2048]{1,0:T(8,128)S(1)}, u32[]{:S(2)}) copy-start(f32[64,2048]{1,0:T(8,128)S(1)} %get-tuple-element.267) | copy-start | bytes 1572868
  92.6 200.0 %copy-start.37 = (f32[32,16,64]{2,1,0:T(8,128)S(1)}, f32[32,16,64]{2,1,0:T(8,128)}, u32[]{:S(2)}) copy-start(f32[32,16,64]{2,1,0:T(8,128)} %param.24) | copy-start | bytes 393220
  369.4 518.7 %all-gather.8.cloned.1.call-start = ((), (), s32[]{:S(2)}) async-start(), calls=%async_computation.3 | async-start | bytes 3145728 | tf_op jit(solution)/shard_map/all_gather | solution.py:188
  381.3 506.9 %all-gather.10.cloned.1.call-start = ((), (), s32[]{:S(2)}) async-start(), calls=%async_computation.4 | async-start | bytes 12255232 | tf_op jit(solution)/shard_map/all_gather | solution.py:191
  382.0 518.6 %all-gather.12.cloned.1.call-start = ((), (), s32[]{:S(2)}) async-start(), calls=%async_computation.5 | async-start | bytes 12255232 | tf_op jit(solution)/shard_map/all_gather | solution.py:196
  382.6 552.7 %reduce-scatter.5.cloned.1.call-start = ((), (), s32[]{:S(2)}) async-start(), calls=%async_computation.6 | async-start | bytes 3145728 | tf_op jit(solution)/shard_map/reduce_scatter | solution.py:204
  382.6 22.1 %collective-permute-start = (bf16[2816,128]{1,0:T(8,128)(2,1)S(1)}, bf16[2816,128]{1,0:T(8,128)(2,1)S(1)}, u32[]{:S(2)}, u32[]{:S(2)}) collective-permute-start(bf16[2816,128]{1,0:T(8,128)(2,1)S(1)} %copy-done.30), channel_id=1, source_target_pairs={{0,2},{2,4},{4,6},{6,8},{8,10},{10,12},{12,14},{14,16},{16,18},{18... | collective-permute-start | bytes 2162696 | tf_op jit(solution)/shard_map/ppermute | solution.py:18
  404.7 35.7 %collective-permute-start.1 = (bf16[2816,128]{1,0:T(8,128)(2,1)S(1)}, bf16[2816,128]{1,0:T(8,128)(2,1)S(1)}, u32[]{:S(2)}, u32[]{:S(2)}) collective-permute-start(bf16[2816,128]{1,0:T(8,128)(2,1)S(1)} %collective-permute-done), channel_id=1, source_target_pairs={{0,2},{2,4},{4,6},{6,8},{8,10},{10,12},{12,14},{14,16},{16,18},{18... | collective-permute-start | bytes 2162696 | tf_op jit(solution)/shard_map/ppermute | solution.py:18
  440.4 34.3 %collective-permute-start.2 = (bf16[2816,128]{1,0:T(8,128)(2,1)S(1)}, bf16[2816,128]{1,0:T(8,128)(2,1)S(1)}, u32[]{:S(2)}, u32[]{:S(2)}) collective-permute-start(bf16[2816,128]{1,0:T(8,128)(2,1)S(1)} %collective-permute-done.1), channel_id=1, source_target_pairs={{0,2},{2,4},{4,6},{6,8},{8,10},{10,12},{12,14},{14,16},{16,18},{18... | collective-permute-start | bytes 2162696 | tf_op jit(solution)/shard_map/ppermute | solution.py:18
  474.8 32.9 %collective-permute-start.3 = (bf16[2816,128]{1,0:T(8,128)(2,1)S(1)}, bf16[2816,128]{1,0:T(8,128)(2,1)S(1)}, u32[]{:S(2)}, u32[]{:S(2)}) collective-permute-start(bf16[2816,128]{1,0:T(8,128)(2,1)S(1)} %collective-permute-done.2), channel_id=1, source_target_pairs={{0,2},{2,4},{4,6},{6,8},{8,10},{10,12},{12,14},{14,16},{16,18},{18... | collective-permute-start | bytes 2162696 | tf_op jit(solution)/shard_map/ppermute | solution.py:18
  507.7 37.2 %collective-permute-start.4 = (bf16[2816,128]{1,0:T(8,128)(2,1)S(1)}, bf16[2816,128]{1,0:T(8,128)(2,1)S(1)}, u32[]{:S(2)}, u32[]{:S(2)}) collective-permute-start(bf16[2816,128]{1,0:T(8,128)(2,1)S(1)} %collective-permute-done.3), channel_id=1, source_target_pairs={{0,2},{2,4},{4,6},{6,8},{8,10},{10,12},{12,14},{14,16},{16,18},{18... | collective-permute-start | bytes 2162696 | tf_op jit(solution)/shard_map/ppermute | solution.py:18
  544.9 37.6 %collective-permute-start.5 = (bf16[2816,128]{1,0:T(8,128)(2,1)S(1)}, bf16[2816,128]{1,0:T(8,128)(2,1)S(1)}, u32[]{:S(2)}, u32[]{:S(2)}) collective-permute-start(bf16[2816,128]{1,0:T(8,128)(2,1)S(1)} %collective-permute-done.4), channel_id=1, source_target_pairs={{0,2},{2,4},{4,6},{6,8},{8,10},{10,12},{12,14},{14,16},{16,18},{18... | collective-permute-start | bytes 2162696 | tf_op jit(solution)/shard_map/ppermute | solution.py:18
  582.5 38.0 %collective-permute-start.6 = (bf16[2816,128]{1,0:T(8,128)(2,1)S(1)}, bf16[2816,128]{1,0:T(8,128)(2,1)S(1)}, u32[]{:S(2)}, u32[]{:S(2)}) collective-permute-start(bf16[2816,128]{1,0:T(8,128)(2,1)S(1)} %collective-permute-done.5), channel_id=1, source_target_pairs={{0,2},{2,4},{4,6},{6,8},{8,10},{10,12},{12,14},{14,16},{16,18},{18... | collective-permute-start | bytes 2162696 | tf_op jit(solution)/shard_map/ppermute | solution.py:18
  620.5 25.9 %collective-permute-start.7 = (bf16[2816,128]{1,0:T(8,128)(2,1)S(1)}, bf16[2816,128]{1,0:T(8,128)(2,1)S(1)}, u32[]{:S(2)}, u32[]{:S(2)}) collective-permute-start(bf16[2816,128]{1,0:T(8,128)(2,1)S(1)} %collective-permute-done.6), channel_id=1, source_target_pairs={{0,2},{2,4},{4,6},{6,8},{8,10},{10,12},{12,14},{14,16},{16,18},{18... | collective-permute-start | bytes 2162696 | tf_op jit(solution)/shard_map/ppermute | solution.py:18
  646.3 26.9 %collective-permute-start.8 = (bf16[2816,128]{1,0:T(8,128)(2,1)S(1)}, bf16[2816,128]{1,0:T(8,128)(2,1)S(1)}, u32[]{:S(2)}, u32[]{:S(2)}) collective-permute-start(bf16[2816,128]{1,0:T(8,128)(2,1)S(1)} %collective-permute-done.7), channel_id=1, source_target_pairs={{0,2},{2,4},{4,6},{6,8},{8,10},{10,12},{12,14},{14,16},{16,18},{18... | collective-permute-start | bytes 2162696 | tf_op jit(solution)/shard_map/ppermute | solution.py:18
  673.3 35.9 %collective-permute-start.9 = (bf16[2816,128]{1,0:T(8,128)(2,1)S(1)}, bf16[2816,128]{1,0:T(8,128)(2,1)S(1)}, u32[]{:S(2)}, u32[]{:S(2)}) collective-permute-start(bf16[2816,128]{1,0:T(8,128)(2,1)S(1)} %collective-permute-done.8), channel_id=1, source_target_pairs={{0,2},{2,4},{4,6},{6,8},{8,10},{10,12},{12,14},{14,16},{16,18},{18... | collective-permute-start | bytes 2162696 | tf_op jit(solution)/shard_map/ppermute | solution.py:18
  709.1 27.9 %collective-permute-start.10 = (bf16[2816,128]{1,0:T(8,128)(2,1)S(1)}, bf16[2816,128]{1,0:T(8,128)(2,1)S(1)}, u32[]{:S(2)}, u32[]{:S(2)}) collective-permute-start(bf16[2816,128]{1,0:T(8,128)(2,1)S(1)} %collective-permute-done.9), channel_id=1, source_target_pairs={{0,2},{2,4},{4,6},{6,8},{8,10},{10,12},{12,14},{14,16},{16,18},{18... | collective-permute-start | bytes 2162696 | tf_op jit(solution)/shard_map/ppermute | solution.py:18
  737.1 37.5 %collective-permute-start.11 = (bf16[2816,128]{1,0:T(8,128)(2,1)S(1)}, bf16[2816,128]{1,0:T(8,128)(2,1)S(1)}, u32[]{:S(2)}, u32[]{:S(2)}) collective-permute-start(bf16[2816,128]{1,0:T(8,128)(2,1)S(1)} %collective-permute-done.10), channel_id=1, source_target_pairs={{0,2},{2,4},{4,6},{6,8},{8,10},{10,12},{12,14},{14,16},{16,18},{18... | collective-permute-start | bytes 2162696 | tf_op jit(solution)/shard_map/ppermute | solution.py:18
  774.5 35.0 %collective-permute-start.12 = (bf16[2816,128]{1,0:T(8,128)(2,1)S(1)}, bf16[2816,128]{1,0:T(8,128)(2,1)S(1)}, u32[]{:S(2)}, u32[]{:S(2)}) collective-permute-start(bf16[2816,128]{1,0:T(8,128)(2,1)S(1)} %collective-permute-done.11), channel_id=1, source_target_pairs={{0,2},{2,4},{4,6},{6,8},{8,10},{10,12},{12,14},{14,16},{16,18},{18... | collective-permute-start | bytes 2162696 | tf_op jit(solution)/shard_map/ppermute | solution.py:18
  809.6 37.2 %collective-permute-start.13 = (bf16[2816,128]{1,0:T(8,128)(2,1)S(1)}, bf16[2816,128]{1,0:T(8,128)(2,1)S(1)}, u32[]{:S(2)}, u32[]{:S(2)}) collective-permute-start(bf16[2816,128]{1,0:T(8,128)(2,1)S(1)} %collective-permute-done.12), channel_id=1, source_target_pairs={{0,2},{2,4},{4,6},{6,8},{8,10},{10,12},{12,14},{14,16},{16,18},{18... | collective-permute-start | bytes 2162696 | tf_op jit(solution)/shard_map/ppermute | solution.py:18
  846.8 15.1 %collective-permute-start.14 = (bf16[2816,128]{1,0:T(8,128)(2,1)S(1)}, bf16[2816,128]{1,0:T(8,128)(2,1)S(1)}, u32[]{:S(2)}, u32[]{:S(2)}) collective-permute-start(bf16[2816,128]{1,0:T(8,128)(2,1)S(1)} %collective-permute-done.13), channel_id=1, source_target_pairs={{0,2},{2,4},{4,6},{6,8},{8,10},{10,12},{12,14},{14,16},{16,18},{18... | collective-permute-start | bytes 2162696 | tf_op jit(solution)/shard_map/ppermute | solution.py:18
  (39 other events, 733.4 us)
Sparse Core Ops, SparseCore 0:
  369.6 7.3 reduce-scatter.2
  381.4 11.8 all-gather.7
  396.0 209.5 all-gather.9
  608.2 221.3 all-gather.11
  928.2 7.0 reduce-scatter.4
